TPU v7x, 32 devices: a whole 2x2x4 slice. The times are simulated.
32 devices in a mesh: sp: 8 (over z, x), tp: 4 (over y, core).
Axes of the slice: x: 2, y: 2, z: 4, core: 2. Of those that a mesh axis runs over, the one named last changes fastest.
Arguments:
- queries: bfloat16 [1536, 1536], P('sp', 'tp'), may hold values from -64 to 64
- latents: bfloat16 [1536, 512], P('sp'), may hold values from -6 to 6
- rope_key: bfloat16 [1536, 32], P('sp'), may hold values from -64 to 64
- w_key: bfloat16 [512, 1024], P(None, 'tp'), may hold values from -0.25 to 0.25
- w_value: bfloat16 [512, 1024], P(None, 'tp'), may hold values from -0.25 to 0.25
- w_out: bfloat16 [1024, 2048], P('tp'), may hold values from -0.59765625 to 0.59765625
- resid: bfloat16 [1536, 2048], P('sp', 'tp'), may hold values from -12 to 12
- gain_mix: float32 [2048], P('tp'), may hold values from 0.1 to 1.9
- w_gate: bfloat16 [2048, 3072], P('sp', 'tp'), may hold values from -0.125 to 0.125
- w_up: bfloat16 [2048, 3072], P('sp', 'tp'), may hold values from -0.125 to 0.125
- w_down: bfloat16 [3072, 2048], P('tp', 'sp'), may hold values from -0.41992188 to 0.41992188
- gain_out: float32 [2048], P('tp'), may hold values from 0.1 to 1.9
Outputs:
- layer_out: bfloat16 [1536, 2048], P('sp', 'tp')
All inputs are finite; a program needn't handle non-finite values.
Results may differ from a plain program's by a relative error of at most 0.014.
Values may be sent and summed in bfloat16 or wider, within the bound.
No kernel may reach another device: no remote copies, remote signals or barrier semaphores. Data moves between devices by JAX's collectives and lax.ppermute only.
A program may use at most 128 MiB of HBM per device.

v0:
```python
import jax
import jax.numpy as jnp
from jax import lax
from jax.sharding import PartitionSpec as P

NOPE = 64
ROPE = 32
VDIM = 64
GRID_W = 64


ROTARY_BASE = 10000.0
NORM_EPSILON = 1e-06
DEEP_ALPHA = 8.0**0.25
HALF_STEP = 0.5


def rotary_tables(positions, rotary_width, grid_width):
    grid_rows = (positions // grid_width).astype(jnp.float32)
    grid_cols = (positions % grid_width).astype(jnp.float32)
    freq_count = rotary_width // 4
    inverse = ROTARY_BASE ** (-jnp.arange(freq_count, dtype=jnp.float32) / freq_count)
    angle_table = jnp.concatenate(
        [grid_rows[:, None] * inverse, grid_cols[:, None] * inverse], axis=-1
    )
    return (jnp.cos(angle_table), jnp.sin(angle_table))


def rotate(vectors, cosine, sine):
    half_width = vectors.shape[-1] // 2
    leading = vectors[..., :half_width].astype(jnp.float32)
    trailing = vectors[..., half_width:].astype(jnp.float32)
    return jnp.concatenate(
        [leading * cosine - trailing * sine, leading * sine + trailing * cosine], axis=-1
    ).astype(jnp.bfloat16)


def attend_block(state, key_block, query_pair):
    maxima, totals, running = state
    key_nope, value_rows, key_rope = key_block
    q_nope, q_rope = query_pair
    head_count = q_nope.shape[1]
    rows_here = key_nope.shape[0]
    key_nope = key_nope.reshape(rows_here, head_count, -1)
    value_rows = value_rows.reshape(rows_here, head_count, -1)
    score_scale = (q_nope.shape[2] + q_rope.shape[2]) ** (-0.5)
    scores = jnp.einsum("qhd,khd->hqk", q_nope, key_nope, preferred_element_type=jnp.float32)
    scores = (
        scores + jnp.einsum("qhd,kd->hqk", q_rope, key_rope, preferred_element_type=jnp.float32)
    ) * score_scale
    new_max = jnp.maximum(maxima, jnp.max(scores, axis=-1))
    weights = jnp.exp(scores - new_max[:, :, None])
    factor = jnp.exp(maxima - new_max)
    totals = totals * factor + jnp.sum(weights, axis=-1)
    update = jnp.einsum(
        "hqk,khd->qhd", weights.astype(jnp.bfloat16), value_rows, preferred_element_type=jnp.float32
    )
    running = running * jnp.transpose(factor)[:, :, None] + update
    return (new_max, totals, running)


def block_length(length):
    block_rows = length
    while block_rows > 2048 and block_rows % 2 == 0:
        block_rows = block_rows // 2
    return block_rows


def fold_keys(state, pieces, query_pair):
    length = pieces[0].shape[0]
    block_rows = block_length(length)
    if block_rows == length:
        return attend_block(state, pieces, query_pair)
    stacked = tuple(
        (member.reshape(length // block_rows, block_rows, member.shape[1]) for member in pieces)
    )

    def one_block(partial_value, key_block):
        return (attend_block(partial_value, key_block, query_pair), None)

    state, unused = lax.scan(one_block, state, stacked)
    return state


def split_norm(rows_in, gain_row):
    width_total = rows_in.shape[1] * lax.axis_size("tp")
    row_sums, squares = lax.psum(
        (jnp.sum(rows_in, axis=1), jnp.sum(rows_in * rows_in, axis=1)), "tp"
    )
    row_mean = row_sums / width_total
    variance = squares / width_total - row_mean * row_mean
    return (
        (rows_in - row_mean[:, None]) * lax.rsqrt(variance + NORM_EPSILON)[:, None] * gain_row
    ).astype(jnp.bfloat16)


def local(
    queries,
    latents,
    rope_key,
    w_key,
    w_value,
    w_out,
    resid,
    gain_mix,
    w_gate,
    w_up,
    w_down,
    gain_out,
):
    local_rows = queries.shape[0]
    head_count = w_key.shape[1] // NOPE
    offset = lax.axis_index("sp") * local_rows
    positions = offset + jnp.arange(local_rows, dtype=jnp.int32)
    cosine, sine = rotary_tables(positions, ROPE, GRID_W)
    key_rot = rotate(rope_key, cosine, sine)
    shaped = queries.reshape(local_rows, head_count, NOPE + ROPE)
    q_nope = shaped[:, :, :NOPE]
    q_rot = rotate(shaped[:, :, NOPE:], cosine[:, None, :], sine[:, None, :])
    query_pair = (q_nope, q_rot)
    start_state = (
        jnp.full((head_count, local_rows), -jnp.inf, jnp.float32),
        jnp.zeros((head_count, local_rows), jnp.float32),
        jnp.zeros((local_rows, head_count, VDIM), jnp.float32),
    )
    quarter = local_rows // lax.axis_size("tp")
    first_row = lax.axis_index("tp") * quarter
    latent_part = lax.dynamic_slice_in_dim(latents, first_row, quarter, 0)
    rotary_part = lax.dynamic_slice_in_dim(key_rot, first_row, quarter, 0)
    latent_all, rotary_all = (
        lax.all_gather(latent_part, "sp", axis=0, tiled=True),
        lax.all_gather(rotary_part, "sp", axis=0, tiled=True),
    )
    pieces = (
        lax.all_gather(latent_all, "tp", axis=0, tiled=True),
        lax.all_gather(rotary_all, "tp", axis=0, tiled=True),
    )
    key_nope = jnp.dot(pieces[0], w_key, preferred_element_type=jnp.float32).astype(jnp.bfloat16)
    value_rows = jnp.dot(pieces[0], w_value, preferred_element_type=jnp.float32).astype(
        jnp.bfloat16
    )
    state = fold_keys(start_state, (key_nope, value_rows, pieces[1]), query_pair)
    maxima, totals, running = state
    heads_out = (
        (running / jnp.transpose(totals)[:, :, None])
        .reshape(local_rows, head_count * VDIM)
        .astype(jnp.bfloat16)
    )
    projected = jnp.dot(heads_out, w_out, preferred_element_type=jnp.float32)
    attn_cols = lax.psum_scatter(
        projected.astype(jnp.bfloat16), "tp", scatter_dimension=1, tiled=True
    ).astype(jnp.float32)
    hidden_in = split_norm(DEEP_ALPHA * resid.astype(jnp.float32) + attn_cols, gain_mix)
    whole_rows = lax.all_gather(hidden_in, "tp", axis=1, tiled=True)
    pieces = (
        lax.all_gather(w_gate, "sp", axis=0, tiled=True),
        lax.all_gather(w_up, "sp", axis=0, tiled=True),
    )
    gate_sum = jnp.dot(whole_rows, pieces[0], preferred_element_type=jnp.float32)
    up_sum = jnp.dot(whole_rows, pieces[1], preferred_element_type=jnp.float32)
    hidden = (jax.nn.silu(gate_sum) * up_sum).astype(jnp.bfloat16)
    down_terms = jnp.dot(
        hidden, lax.all_gather(w_down, "sp", axis=1, tiled=True), preferred_element_type=jnp.float32
    )
    mixer_cols = lax.psum_scatter(
        down_terms.astype(jnp.bfloat16), "tp", scatter_dimension=1, tiled=True
    ).astype(jnp.float32)
    return split_norm(DEEP_ALPHA * hidden_in.astype(jnp.float32) + HALF_STEP * mixer_cols, gain_out)


def solution(mesh):
    placed = (
        P("sp", "tp"),
        P("sp", None),
        P("sp", None),
        P(None, "tp"),
        P(None, "tp"),
        P("tp", None),
        P("sp", "tp"),
        P("tp"),
        P("sp", "tp"),
        P("sp", "tp"),
        P("tp", "sp"),
        P("tp"),
    )
    return jax.shard_map(
        local, mesh=mesh, in_specs=placed, out_specs=P("sp", "tp"), check_vma=False
    )
```

profile of v0, /device:TPU:0, one launch (start us, length us, event | category | flops | bytes accessed | tf_op | source)
XLA Modules:
  0.0 324.2 jit_solution(2186468816205035295)
XLA Ops:
  7.4 0.0 all-gather.6.cloned.1.call-start
  7.4 0.9 constant_dynamic-slice_fusion
  8.3 34.8 %all_gather.24 = bf16[384,512]{1,0:T(8,128)(2,1)} all-gather(bf16[48,512]{1,0:T(8,128)(2,1)S(1)} %constant_dynamic-slice_fusion), channel_id=1, replica_groups=mesh['sp'=8,'tp'=4] {'sp'}, dimensions={0}, use_global_device_ids=true | all-gather | bytes 442368 | tf_op jit(solution)/shard_map/all_gather | solution.py:131
  43.1 0.0 all-gather.6.cloned.1.call-update
  43.1 0.0 reduce-scatter.3.cloned.1.call-start
  43.2 0.1 broadcast_multiply_fusion.1
  43.3 0.8 fusion.40
  44.1 0.1 fusion.44
  44.2 30.5 %all-gather = bf16[8,48,32]{1,2,0:T(8,128)(2,1)S(1)} all-gather(bf16[1,48,32]{1,2,0:T(8,128)(2,1)S(1)} %fusion.44), channel_id=1, replica_groups=mesh['sp'=8,'tp'=4] {'sp'}, dimensions={0}, use_global_device_ids=true | all-gather | bytes 27648 | tf_op jit(solution)/shard_map/all_gather | solution.py:132
  74.7 0.1 reshape.118
  74.9 1.0 copy.16
  75.9 5.3 %all_gather.27 = bf16[1536,32]{0,1:T(8,128)(2,1)S(1)} all-gather(bf16[384,32]{0,1:T(8,128)(2,1)S(1)} %reshape.118), channel_id=1, replica_groups=mesh['sp'=8,'tp'=4] {'tp'}, dimensions={0}, use_global_device_ids=true | all-gather | bytes 122880 | tf_op jit(solution)/shard_map/all_gather | solution.py:136
  81.3 2.9 fusion.28
  84.2 2.0 convolution_convert_fusion.1
  86.2 3.3 %fusion.50 = (f32[4,192]{1,0:T(4,128)S(1)}, f32[4,192,1536]{2,1,0:T(8,128)S(1)}) fusion(f32[1536,192,4]{0,1,2:T(8,128)} %fusion.28, bf16[1536,4,64]{0,2,1:T(8,128)(2,1)S(1)} %bitcast.45, bf16[192,4,96]{0,2,1:T(8,128)(2,1)S(1)} %bitcast.47), kind=kOutput, calls=%fused_computation.82 | convolution fusion | flops 154533120 | bytes 10357760 | tf_op jit(solution)/shard_map/qhd,khd->hqk/dot_general | solution.py:47
  89.5 0.0 copy-start.1
  89.5 0.0 copy-start.4
  89.6 0.8 fusion.1
  90.3 0.6 copy-done.1
  90.9 0.0 copy-done.4
  90.9 0.6 convolution_convert_fusion
  91.6 1.0 fusion.16
  92.6 0.0 copy-start.5
  92.6 1.3 convolution_convert_fusion.3
  93.9 0.0 reduce-scatter.3.cloned.1.call-update
  93.9 0.0 all-gather.8.cloned.1.call-start
  94.0 0.5 all-gather.8.cloned.1.call-update
  94.5 0.0 all-gather.10.cloned.1.call-start
  94.6 0.5 all-gather.10.cloned.1.call-update
  95.1 0.0 all-gather.12.cloned.1.call-start
  95.1 0.5 all-gather.12.cloned.1.call-update
  95.7 0.0 reduce-scatter.5.cloned.1.call-start
  95.7 22.5 %reduce-scatter.3.cloned.1.call-done = bf16[192,512]{1,0:T(8,128)(2,1)} async-done(((bf16[192,2048]{1,0:T(8,128)(2,1)}), bf16[192,512]{1,0:T(8,128)(2,1)}) %reduce-scatter.3.cloned.1.call-update) | async-done | bytes 196624 | tf_op jit(solution)/shard_map/reduce_scatter | solution.py:150
  118.3 1.1 fusion.24
  119.4 5.8 %all-reduce.1 = (f32[192]{0:T(256)S(1)}, f32[192]{0:T(256)S(1)}) all-reduce(f32[192]{0:T(256)S(1)} %get-tuple-element.8, f32[192]{0:T(256)S(1)} %get-tuple-element.7), channel_id=1, replica_groups=mesh['sp'=8,'tp'=4] {'tp'}, use_global_device_ids=true, to_apply=%region_6.7 | all-reduce | flops 384 | bytes 3072 | tf_op jit(solution)/shard_map/psum | solution.py:87
  125.2 1.1 multiply_convert_fusion.1
  126.2 8.3 %all_gather.28 = bf16[192,2048]{1,0:T(8,128)(2,1)S(1)} all-gather(bf16[192,512]{1,0:T(8,128)(2,1)S(1)} %multiply_convert_fusion.1), channel_id=1, replica_groups=mesh['sp'=8,'tp'=4] {'tp'}, dimensions={1}, use_global_device_ids=true | all-gather | bytes 983040 | tf_op jit(solution)/shard_map/all_gather | solution.py:154
  134.5 22.9 %all-gather.8.cloned.1.call-done = bf16[2048,768]{1,0:T(8,128)(2,1)} async-done(((bf16[256,768]{1,0:T(8,128)(2,1)}), bf16[2048,768]{1,0:T(8,128)(2,1)}) %all-gather.8.cloned.1.call-update) | async-done | bytes 3145744 | tf_op jit(solution)/shard_map/all_gather | solution.py:156
  157.5 2.7 fusion.51
  160.2 0.0 copy-start.6
  160.2 58.0 %all-gather.10.cloned.1.call-done = bf16[2048,768]{1,0:T(8,128)(2,1)} async-done(((bf16[256,768]{1,0:T(8,128)(2,1)}), bf16[2048,768]{1,0:T(8,128)(2,1)}) %all-gather.10.cloned.1.call-update) | async-done | bytes 3145744 | tf_op jit(solution)/shard_map/all_gather | solution.py:157
  218.1 63.1 %all-gather.12.cloned.1.call-done = bf16[768,2048]{1,0:T(8,128)(2,1)} async-done(((bf16[768,256]{1,0:T(8,128)(2,1)}), bf16[768,2048]{1,0:T(8,128)(2,1)}) %all-gather.12.cloned.1.call-update) | async-done | bytes 3145744 | tf_op jit(solution)/shard_map/all_gather | solution.py:163
  281.2 5.4 %convolution_convert_fusion.2 = bf16[192,2048]{1,0:T(8,128)(2,1)} fusion(bf16[768,2048]{1,0:T(8,128)(2,1)} %all-gather.12.cloned.1.call-done, bf16[192,2048]{1,0:T(8,128)(2,1)S(1)} %all_gather.28, bf16[2048,768]{1,0:T(8,128)(2,1)} %all-gather.10.cloned.1.call-done, f32[192,768]{1,0:T(8,128)S(1)} %fusion.51), kind=kOutput, calls=%fused_computation.7 | convolution fusion | flops 1209237504 | bytes 8454144 | tf_op jit(solution)/shard_map/dot_general | solution.py:162
  286.6 0.0 reduce-scatter.5.cloned.1.call-update
  286.6 21.6 %reduce-scatter.5.cloned.1.call-done = bf16[192,512]{1,0:T(8,128)(2,1)} async-done(((bf16[192,2048]{1,0:T(8,128)(2,1)}), bf16[192,512]{1,0:T(8,128)(2,1)}) %reduce-scatter.5.cloned.1.call-update) | async-done | bytes 196624 | tf_op jit(solution)/shard_map/reduce_scatter | solution.py:165
  308.2 1.1 fusion.26
  309.3 5.8 %all-reduce = (f32[192]{0:T(256)S(1)}, f32[192]{0:T(256)S(1)}) all-reduce(f32[192]{0:T(256)S(1)} %get-tuple-element.6, f32[192]{0:T(256)S(1)} %get-tuple-element.5), channel_id=1, replica_groups=mesh['sp'=8,'tp'=4] {'tp'}, use_global_device_ids=true, to_apply=%region_11.12 | all-reduce | flops 384 | bytes 3072 | tf_op jit(solution)/shard_map/psum | solution.py:87
  315.1 1.7 multiply_convert_fusion
  (17 shorter events, 0.1 us)
Async XLA Ops:
  7.4 85.2 %copy-start = (bf16[256,2048]{1,0:T(8,128)(2,1)S(1)}, bf16[256,2048]{1,0:T(8,128)(2,1)}, u32[]{:S(2)}) copy-start(bf16[256,2048]{1,0:T(8,128)(2,1)} %param.17) | copy-start | bytes 3145732
  7.4 76.8 %all-gather.6.cloned.1.call-start = ((), (), s32[]{:S(2)}) async-start(), calls=%async_computation.2 | async-start | bytes 1966080 | tf_op jit(solution)/shard_map/all_gather | solution.py:135
  43.1 41.1 %copy-start.3 = (bf16[512,256]{1,0:T(8,128)(2,1)S(1)}, bf16[512,256]{1,0:T(8,128)(2,1)}, u32[]{:S(2)}) copy-start(bf16[512,256]{1,0:T(8,128)(2,1)} %param.15) | copy-start | bytes 786436
  43.1 75.1 %reduce-scatter.3.cloned.1.call-start = ((), (), s32[]{:S(2)}) async-start(), calls=%async_computation.3 | async-start | bytes 983040 | tf_op jit(solution)/shard_map/reduce_scatter | solution.py:150
  89.5 1.4 copy-start.1
  89.5 1.4 copy-start.4
  92.6 25.7 %copy-start.2 = (bf16[192,512]{1,0:T(8,128)(2,1)S(1)}, bf16[192,512]{1,0:T(8,128)(2,1)}, u32[]{:S(2)}) copy-start(bf16[192,512]{1,0:T(8,128)(2,1)} %param.18) | copy-start | bytes 589828
  92.6 32.6 %copy-start.5 = (f32[512]{0:T(512)S(1)}, f32[512]{0:T(512)}, u32[]{:S(2)}) copy-start(f32[512]{0:T(512)} %param.19) | copy-start | bytes 6148
  93.9 63.6 %all-gather.8.cloned.1.call-start = ((), (), s32[]{:S(2)}) async-start(), calls=%async_computation.4 | async-start | bytes 3538944 | tf_op jit(solution)/shard_map/all_gather | solution.py:156
  94.5 123.6 %all-gather.10.cloned.1.call-start = ((), (), s32[]{:S(2)}) async-start(), calls=%async_computation.5 | async-start | bytes 3538944 | tf_op jit(solution)/shard_map/all_gather | solution.py:157
  95.1 186.1 %all-gather.12.cloned.1.call-start = ((), (), s32[]{:S(2)}) async-start(), calls=%async_computation.6 | async-start | bytes 3538944 | tf_op jit(solution)/shard_map/all_gather | solution.py:163
  95.7 212.5 %reduce-scatter.5.cloned.1.call-start = ((), (), s32[]{:S(2)}) async-start(), calls=%async_computation.7 | async-start | bytes 983040 | tf_op jit(solution)/shard_map/reduce_scatter | solution.py:165
  160.2 154.9 %copy-start.6 = (f32[512]{0:T(512)S(1)}, f32[512]{0:T(512)}, u32[]{:S(2)}) copy-start(f32[512]{0:T(512)} %param.23) | copy-start | bytes 6148
Sparse Core Ops, SparseCore 0:
  43.3 20.5 all-gather.5
  94.0 24.1 reduce-scatter.2
  286.8 21.3 reduce-scatter.4
Sparse Core Ops, SparseCore 1:
  96.6 60.8 all-gather.7
  159.5 58.5 all-gather.9
  220.1 61.1 all-gather.11
where the time goes:
time: 325 us; the launch traced here: 324 us
  waiting for transfers between devices  190 us (58%)
  blocking collectives  90.5 us (28%)
  matrix products  19.2 us (6%)
  between operations  14.9 us (5%)
  other arithmetic  6.87 us (2%)
    all_gather x1, waiting for transfers between devices, local(): lax.all_gather(w_down, 'sp', axis=1, tiled=True)  63.1 us
    all_gather x1, waiting for transfers between devices, local(): lax.all_gather(w_up, 'sp', axis=0, tiled=True)  58 us
    all_gather x1, blocking collectives, local(): lax.all_gather(latent_part, 'sp', axis=0, tiled=True)  34.8 us
    all_gather x1, blocking collectives, local(): lax.all_gather(rotary_part, 'sp', axis=0, tiled=True)  30.5 us
    all_gather x1, waiting for transfers between devices, local(): lax.all_gather(w_gate, 'sp', axis=0, tiled=True)  22.9 us
    reduce_scatter x1, waiting for transfers between devices, local(): lax.psum_scatter(projected.astype(jnp.bfloat16), 'tp', scatter_dimension=...  22.5 us
    reduce_scatter x1, waiting for transfers between devices, local(): lax.psum_scatter(down_terms.astype(jnp.bfloat16), 'tp', scatter_dimension...  21.6 us
    psum x2, blocking collectives, split_norm(): lax.psum((jnp.sum(rows_in, axis=1), jnp.sum(rows_in * rows_in, axis=1)),...  11.5 us
  transfers between devices with their start and end apart: 6, of which 5 were waited for; matrix products, arithmetic and copies ran while one was open for 3% of the time, Pallas kernels for 0%

commit v1 on v0

--- a/solution.py
+++ b/solution.py
@@ -1,6 +1,11 @@
+import functools
+
 import jax
 import jax.numpy as jnp
 from jax import lax
+from jax.experimental import pallas as pl
+from jax.experimental.pallas import tpu as pltpu
+
 from jax.sharding import PartitionSpec as P
 
 NOPE = 64
@@ -78,7 +83,7 @@
     def one_block(partial_value, key_block):
         return (attend_block(partial_value, key_block, query_pair), None)
 
-    state, unused = lax.scan(one_block, state, stacked)
+    state, _ = lax.scan(one_block, state, stacked)
     return state
 
 
@@ -140,7 +145,7 @@
         jnp.bfloat16
     )
     state = fold_keys(start_state, (key_nope, value_rows, pieces[1]), query_pair)
-    maxima, totals, running = state
+    _, totals, running = state
     heads_out = (
         (running / jnp.transpose(totals)[:, :, None])
         .reshape(local_rows, head_count * VDIM)
@@ -166,6 +171,575 @@
         down_terms.astype(jnp.bfloat16), "tp", scatter_dimension=1, tiled=True
     ).astype(jnp.float32)
     return split_norm(DEEP_ALPHA * hidden_in.astype(jnp.float32) + HALF_STEP * mixer_cols, gain_out)
+
+
+RING = 4
+PAIR = 2
+LANES = 128
+BOTH = ("sp", "tp")
+VMEM = pl.BlockSpec(memory_space=pltpu.VMEM)
+HBM = pl.BlockSpec(memory_space=pl.ANY)
+PARAMS = pltpu.CompilerParams(vmem_limit_bytes=20 * 1024 * 1024)
+
+
+def fits_plan(mesh):
+    return mesh.shape["sp"] == RING * PAIR and mesh.shape["tp"] == PAIR * PAIR
+
+
+def sp_index(r, p):
+    return (r // PAIR) * PAIR * PAIR + p * PAIR + r % PAIR
+
+
+def move(array, where):
+    pairs = []
+    for r in range(RING):
+        for p in range(PAIR):
+            for y in range(PAIR):
+                for c in range(PAIR):
+                    target = where(r, p, y, c)
+                    if target is None:
+                        continue
+                    to_r, to_p, to_y, to_c = target
+                    here = sp_index(r, p) * PAIR * PAIR + y * PAIR + c
+                    there = sp_index(to_r, to_p) * PAIR * PAIR + to_y * PAIR + to_c
+                    pairs.append((here, there))
+    return lax.ppermute(array, BOTH, pairs)
+
+
+def flip(array, dr=0, dp=0, dy=0, dc=0):
+    return move(array, lambda r, p, y, c: (r ^ dr, p ^ dp, y ^ dy, c ^ dc))
+
+
+def partner(array):
+    return flip(array, dc=1)
+
+
+def exchange_halves(array):
+    return move(array, lambda r, p, y, c: (r, c, y, p) if c != p else None)
+
+
+ROUNDS = ((0, 0), (0, 1), (1, 0), (1, 1))
+
+
+def spread(array, dy, k):
+    return move(array, lambda r, p, y, c: (r, c ^ k, y ^ dy, p))
+
+
+def coordinates():
+    sp = lax.axis_index("sp")
+    tp = lax.axis_index("tp")
+    ring = (sp // (PAIR * PAIR)) * PAIR + sp % PAIR
+    return (ring, (sp // PAIR) % PAIR, tp // PAIR, tp % PAIR)
+
+
+def other(bit):
+    return 1 - bit
+
+
+def round_block(dy, k, p, y):
+    row = other(y) if dy else y
+    column = other(p) if k else p
+    return row * PAIR + column
+
+
+def query_tiles(queries, cosine, sine):
+    rows = queries.shape[0]
+    half = ROPE // 2
+    heads_per_tile = LANES // NOPE
+    tiles = []
+    for head in range(queries.shape[1] // (NOPE + ROPE)):
+        start = head * (NOPE + ROPE)
+        plain = queries[:, start : start + NOPE]
+        leading = queries[:, start + NOPE : start + NOPE + half]
+        trailing = queries[:, start + NOPE + half : start + NOPE + ROPE]
+        part = head % heads_per_tile
+        pieces = [plain]
+        if part:
+            pieces.insert(0, jnp.zeros((rows, part * NOPE), jnp.float32))
+        if part < heads_per_tile - 1:
+            pieces.append(jnp.zeros((rows, LANES - (part + 1) * NOPE), jnp.float32))
+        pieces.append(leading * cosine - trailing * sine)
+        pieces.append(leading * sine + trailing * cosine)
+        pieces.append(jnp.zeros((rows, LANES - ROPE), jnp.float32))
+        tiles.append(jnp.concatenate(pieces, axis=1).astype(jnp.bfloat16))
+    return tiles
+
+
+def attention_kernel(scale, n_blocks, *refs):
+    first = refs[:3]
+    blocks = refs[3 : 3 + n_blocks]
+    weights = refs[3 + n_blocks : 5 + n_blocks]
+    out_hbm, k_scr, v_scr, x_scr, q_ref, cos_ref, sin_ref, wk_ref, wv_ref, out_ref, sems = refs[
+        5 + n_blocks :
+    ]
+    rank = wk_ref.shape[0]
+    tiles = wk_ref.shape[1] // LANES
+    copies = []
+    early = []
+    for at, (ref, scr) in enumerate(zip(first, (q_ref, cos_ref, sin_ref))):
+        early.append(pltpu.make_async_copy(ref, scr, sems.at[n_blocks + at]))
+    for at, (ref, scr) in enumerate(zip(weights, (wk_ref, wv_ref))):
+        copies.append(pltpu.make_async_copy(ref, scr, sems.at[n_blocks + 3 + at]))
+    for copy in early + copies:
+        copy.start()
+    offset = 0
+    for at, ref in enumerate(blocks):
+        rows = ref.shape[0]
+        copy = pltpu.make_async_copy(ref, x_scr.at[pl.ds(offset, rows)], sems.at[at])
+        copy.start()
+        copies.append(copy)
+        offset += rows
+    for copy in early:
+        copy.wait()
+    q_tiles = query_tiles(q_ref[...].astype(jnp.float32), cos_ref[...], sin_ref[...])
+    for copy in copies:
+        copy.wait()
+    lat = x_scr[:, :rank]
+    keys = jnp.dot(lat, wk_ref[...], preferred_element_type=jnp.float32).astype(jnp.bfloat16)
+    for tile in range(tiles):
+        k_scr[tile, :, :LANES] = keys[:, tile * LANES : (tile + 1) * LANES]
+        k_scr[tile, :, LANES:] = x_scr[:, rank:]
+    v_scr[...] = jnp.dot(lat, wv_ref[...], preferred_element_type=jnp.float32).astype(jnp.bfloat16)
+    heads_per_tile = LANES // NOPE
+    for tile in range(tiles):
+        merged = None
+        for part in range(heads_per_tile):
+            scores = lax.dot_general(
+                q_tiles[tile * heads_per_tile + part],
+                k_scr[tile],
+                (((1,), (1,)), ((), ())),
+                preferred_element_type=jnp.float32,
+            )
+            top = jnp.max(scores, axis=-1, keepdims=True)
+            weights = jnp.exp((scores - top) * scale)
+            total = jnp.sum(weights, axis=-1, keepdims=True)
+            update = jnp.dot(
+                weights.astype(jnp.bfloat16),
+                v_scr[:, tile * LANES : (tile + 1) * LANES],
+                preferred_element_type=jnp.float32,
+            )
+            update = update / total
+            lane = lax.broadcasted_iota(jnp.int32, update.shape, 1)
+            mine = (lane >= part * NOPE) & (lane < (part + 1) * NOPE)
+            merged = update if merged is None else jnp.where(mine, update, merged)
+        out_ref[:, tile * LANES : (tile + 1) * LANES] = merged.astype(jnp.bfloat16)
+    done = pltpu.make_async_copy(out_ref, out_hbm, sems.at[0])
+    done.start()
+    done.wait()
+
+
+def attend(queries, cosine, sine, blocks, w_key, w_value):
+    keys = sum(block.shape[0] for block in blocks)
+    tiles = w_key.shape[1] // LANES
+    rows = queries.shape[0]
+    return pl.pallas_call(
+        functools.partial(attention_kernel, (NOPE + ROPE) ** (-0.5), len(blocks)),
+        out_shape=jax.ShapeDtypeStruct((rows, w_value.shape[1]), jnp.bfloat16),
+        in_specs=[HBM] * (len(blocks) + 5),
+        out_specs=HBM,
+        scratch_shapes=[
+            pltpu.VMEM((tiles, keys, 2 * LANES), jnp.bfloat16),
+            pltpu.VMEM((keys, w_value.shape[1]), jnp.bfloat16),
+            pltpu.VMEM((keys, blocks[0].shape[1]), jnp.bfloat16),
+            pltpu.VMEM(queries.shape, queries.dtype),
+            pltpu.VMEM(cosine.shape, cosine.dtype),
+            pltpu.VMEM(sine.shape, sine.dtype),
+            pltpu.VMEM(w_key.shape, w_key.dtype),
+            pltpu.VMEM(w_value.shape, w_value.dtype),
+            pltpu.VMEM((rows, w_value.shape[1]), jnp.bfloat16),
+            pltpu.SemaphoreType.DMA((len(blocks) + 5,)),
+        ],
+        compiler_params=PARAMS,
+        name="attend",
+    )(queries, cosine, sine, *blocks, w_key, w_value)
+
+
+def mix_kernel(*refs):
+    heads = refs[0:4]
+    w_refs = refs[4:8]
+    resid_refs = refs[8:12]
+    out_hbm, hid_ref, h_scr, w_scr, in_scr, res_scr, gain_scr, sems = refs[12:]
+    _, p, y, c = coordinates()
+    turned = (p + c) % PAIR
+    small = []
+    large = []
+    for j in range(4):
+        slot = j + turned * (1 - 2 * (j % PAIR))
+        small.append(pltpu.make_async_copy(resid_refs[j], in_scr.at[j], sems.at[0, j]))
+        large.append(pltpu.make_async_copy(heads[j], h_scr.at[j], sems.at[1, j]))
+        large.append(pltpu.make_async_copy(w_refs[j], w_scr.at[slot], sems.at[2, j]))
+    for copy in small + large:
+        copy.start()
+    for copy in small:
+        copy.wait()
+    rows = hid_ref.shape[0]
+    width = resid_refs[0].shape[1]
+    for j, (dy, k) in enumerate(ROUNDS):
+        columns = pl.ds(pl.multiple_of(round_block(dy, k, p, y) * width, width), width)
+        res_scr[:, columns] = DEEP_ALPHA * in_scr[j, :rows, :].astype(jnp.float32)
+        gains = in_scr[j, rows:, :].astype(jnp.float32)
+        gain_scr[:, columns] = gains[0:1] + gains[1:2] + gains[2:3]
+    for copy in large:
+        copy.wait()
+    chunk = rows // 4
+    outs = []
+    for start in range(0, rows, chunk):
+        span = slice(start, start + chunk)
+        mixed = res_scr[span, :]
+        for j in range(4):
+            mixed = mixed + jnp.dot(h_scr[j, span, :], w_scr[j], preferred_element_type=jnp.float32)
+        mean = jnp.mean(mixed, axis=1, keepdims=True)
+        variance = jnp.mean(mixed * mixed, axis=1, keepdims=True) - mean * mean
+        hid_ref[span, :] = (
+            (mixed - mean) * lax.rsqrt(variance + NORM_EPSILON) * gain_scr[...]
+        ).astype(jnp.bfloat16)
+        part = pl.ds(start, chunk)
+        copy = pltpu.make_async_copy(hid_ref.at[part], out_hbm.at[part], sems.at[3, len(outs)])
+        copy.start()
+        outs.append(copy)
+    for copy in outs:
+        copy.wait()
+
+
+def mix(heads, w_pieces, resid_pieces):
+    rows, share = heads[0].shape
+    depth, width_total = w_pieces[0].shape
+    return pl.pallas_call(
+        mix_kernel,
+        out_shape=jax.ShapeDtypeStruct((rows, width_total), jnp.bfloat16),
+        in_specs=[HBM] * 12,
+        out_specs=HBM,
+        scratch_shapes=[
+            pltpu.VMEM((rows, width_total), jnp.bfloat16),
+            pltpu.VMEM((4, rows, share), jnp.bfloat16),
+            pltpu.VMEM((4, depth, width_total), jnp.bfloat16),
+            pltpu.VMEM((4,) + resid_pieces[0].shape, jnp.bfloat16),
+            pltpu.VMEM((rows, width_total), jnp.float32),
+            pltpu.VMEM((1, width_total), jnp.float32),
+            pltpu.SemaphoreType.DMA((4, 4)),
+        ],
+        compiler_params=PARAMS,
+        name="mix",
+    )(*heads, *w_pieces, *resid_pieces)
+
+
+def homes(r):
+    high = r // PAIR
+    low = r % PAIR
+    return ((high, low), (high, other(low)), (other(high), low), (other(high), other(low)))
+
+
+def up_kernel(own_ref, got_ref, *refs):
+    gates = refs[:4]
+    ups = refs[4:8]
+    out_hbm, out_ref, h_scr, g_scr, u_scr, sems = refs[8:]
+    r, _, _, c = coordinates()
+    depth, units = gates[0].shape
+    rows = own_ref.shape[0]
+    copies = []
+    for at in range(4):
+        span = pl.ds(at * depth, depth)
+        copies.append(pltpu.make_async_copy(gates[at], g_scr.at[span], sems.at[0, at]))
+    for at in range(4):
+        span = pl.ds(at * depth, depth)
+        copies.append(pltpu.make_async_copy(ups[at], u_scr.at[span], sems.at[1, at]))
+    for at, (row, column) in enumerate(homes(r)):
+        block = row * PAIR * PAIR + c * PAIR + column
+        columns = pl.ds(pl.multiple_of(block * depth, depth), depth)
+        span = pl.ds(at * depth, depth)
+        for side, ref in enumerate((own_ref, got_ref)):
+            copies.append(
+                pltpu.make_async_copy(
+                    ref.at[:, columns],
+                    h_scr.at[pl.ds(side * rows, rows), span],
+                    sems.at[2 + side, at],
+                )
+            )
+    for copy in copies:
+        copy.start()
+    for copy in copies[:4] + copies[8:]:
+        copy.wait()
+    hid = h_scr[...]
+    out_ref[:, :units] = jnp.dot(hid, g_scr[...], preferred_element_type=jnp.float32).astype(
+        jnp.bfloat16
+    )
+    outs = []
+    for side in range(2):
+        columns = pl.ds(side * units, units)
+        outs.append(
+            pltpu.make_async_copy(
+                out_ref.at[:, columns], out_hbm.at[:, columns], sems.at[4, side]
+            )
+        )
+    outs[0].start()
+    for copy in copies[4:8]:
+        copy.wait()
+    out_ref[:, units:] = jnp.dot(hid, u_scr[...], preferred_element_type=jnp.float32).astype(
+        jnp.bfloat16
+    )
+    outs[1].start()
+    for copy in outs:
+        copy.wait()
+
+
+def feed_up(own, got, gates, ups):
+    rows = own.shape[0]
+    depth, units = gates[0].shape
+    return pl.pallas_call(
+        up_kernel,
+        out_shape=jax.ShapeDtypeStruct((PAIR * rows, 2 * units), jnp.bfloat16),
+        in_specs=[HBM] * 10,
+        out_specs=HBM,
+        scratch_shapes=[
+            pltpu.VMEM((PAIR * rows, 2 * units), jnp.bfloat16),
+            pltpu.VMEM((PAIR * rows, 4 * depth), jnp.bfloat16),
+            pltpu.VMEM((4 * depth, units), jnp.bfloat16),
+            pltpu.VMEM((4 * depth, units), jnp.bfloat16),
+            pltpu.SemaphoreType.DMA((5, 4)),
+        ],
+        compiler_params=PARAMS,
+        name="feed_up",
+    )(own, got, *gates, *ups)
+
+
+def down_kernel(own_ref, got_ref, *refs):
+    downs = refs[:4]
+    outs = refs[4:8]
+    o_scr, a_scr, d_scr, own_scr, got_scr, sems = refs[8:]
+    r, p, y, c = coordinates()
+    depth = downs[0].shape[1]
+    rows, units = a_scr.shape[1:]
+    copies = []
+    for at, (row, column) in enumerate(homes(r)):
+        columns = pl.ds(pl.multiple_of(column * depth, depth), depth)
+        copies.append(
+            pltpu.make_async_copy(downs[at], d_scr.at[row, :, columns], sems.at[at])
+        )
+    inputs = [
+        pltpu.make_async_copy(own_ref, own_scr, sems.at[4]),
+        pltpu.make_async_copy(got_ref, got_scr, sems.at[5]),
+    ]
+    for copy in inputs + copies:
+        copy.start()
+    for copy in inputs:
+        copy.wait()
+    for side in range(2):
+        mine = pl.ds(side * rows, rows)
+        theirs = pl.ds((1 - side) * rows, rows)
+        gate = own_scr[mine, :units].astype(jnp.float32) + got_scr[theirs, :units].astype(
+            jnp.float32
+        )
+        up = own_scr[mine, units:].astype(jnp.float32) + got_scr[theirs, units:].astype(
+            jnp.float32
+        )
+        group = c if side == 0 else other(c)
+        a_scr[group] = (gate / (1.0 + jnp.exp(-gate)) * up).astype(jnp.bfloat16)
+    for copy in copies:
+        copy.wait()
+    stores = []
+    for j, (dy, dp) in enumerate(ROUNDS):
+        group = other(p) if dp else p
+        row = other(y) if dy else y
+        o_scr[j] = jnp.dot(a_scr[group], d_scr[row], preferred_element_type=jnp.float32).astype(
+            jnp.bfloat16
+        )
+        copy = pltpu.make_async_copy(o_scr.at[j], outs[j], sems.at[6 + j])
+        copy.start()
+        stores.append(copy)
+    for copy in stores:
+        copy.wait()
+
+
+def feed_down(own, got, downs):
+    rows = own.shape[0] // PAIR
+    units, depth = downs[0].shape
+    block = jax.ShapeDtypeStruct((rows, PAIR * depth), jnp.bfloat16)
+    return pl.pallas_call(
+        down_kernel,
+        out_shape=(block,) * 4,
+        in_specs=[HBM] * 6,
+        out_specs=(HBM,) * 4,
+        scratch_shapes=[
+            pltpu.VMEM((4, rows, PAIR * depth), jnp.bfloat16),
+            pltpu.VMEM((PAIR, rows, units), jnp.bfloat16),
+            pltpu.VMEM((PAIR, units, PAIR * depth), jnp.bfloat16),
+            pltpu.VMEM(own.shape, jnp.bfloat16),
+            pltpu.VMEM(own.shape, jnp.bfloat16),
+            pltpu.SemaphoreType.DMA((10,)),
+        ],
+        compiler_params=PARAMS,
+        name="feed_down",
+    )(own, got, *downs)
+
+
+def sum_kernel(own_ref, got_ref, *refs):
+    terms = refs[:4]
+    pre_ref, stat_ref, t_scr, h_scr, sems = refs[4:]
+    _, p, y, c = coordinates()
+    rows, width = pre_ref.shape
+    copies = []
+    for j in range(4):
+        copy = pltpu.make_async_copy(terms[j], t_scr.at[j], sems.at[j])
+        copy.start()
+        copies.append(copy)
+    columns = pl.ds(pl.multiple_of((y * PAIR + c) * width, width), width)
+    for side, ref in enumerate((own_ref, got_ref)):
+        copy = pltpu.make_async_copy(ref.at[:, columns], h_scr.at[side], sems.at[4 + side])
+        copy.start()
+        copies.append(copy)
+    for copy in copies:
+        copy.wait()
+    total = jnp.zeros((rows, width), jnp.float32)
+    for j in range(4):
+        total = total + t_scr[j].astype(jnp.float32)
+    skip = h_scr[(p + c) % PAIR].astype(jnp.float32)
+    pre = DEEP_ALPHA * skip + HALF_STEP * total
+    pre_ref[...] = pre
+    lane = lax.broadcasted_iota(jnp.int32, (rows, LANES), 1)
+    sums = jnp.sum(pre, axis=1, keepdims=True)
+    squares = jnp.sum(pre * pre, axis=1, keepdims=True)
+    table = jnp.where(lane == 0, sums, jnp.where(lane == 1, squares, 0.0))
+    stat_ref[...] = jnp.transpose(table)[: stat_ref.shape[0], :]
+
+
+def add_up(own, got, terms):
+    rows, width = terms[0].shape
+    return pl.pallas_call(
+        sum_kernel,
+        out_shape=(
+            jax.ShapeDtypeStruct((rows, width), jnp.float32),
+            jax.ShapeDtypeStruct((8, rows), jnp.float32),
+        ),
+        in_specs=[HBM] * 6,
+        out_specs=(VMEM,) * 2,
+        scratch_shapes=[
+            pltpu.VMEM((4, rows, width), jnp.bfloat16),
+            pltpu.VMEM((2, rows, width), jnp.bfloat16),
+            pltpu.SemaphoreType.DMA((6,)),
+        ],
+        compiler_params=PARAMS,
+        name="add_up",
+    )(own, got, *terms)
+
+
+def norm_kernel(width_total, pre_ref, a_ref, b_ref, c_ref, d_ref, gain_ref, out_ref):
+    stats = a_ref[...] + b_ref[...] + c_ref[...] + d_ref[...]
+    tall = jnp.concatenate(
+        [stats, jnp.zeros((LANES - stats.shape[0], stats.shape[1]), jnp.float32)], axis=0
+    )
+    table = jnp.transpose(tall)
+    mean = table[:, 0:1] / width_total
+    variance = table[:, 1:2] / width_total - mean * mean
+    out_ref[...] = (
+        (pre_ref[...] - mean) * lax.rsqrt(variance + NORM_EPSILON) * gain_ref[...]
+    ).astype(jnp.bfloat16)
+
+
+def finish(pre, stats, gain):
+    return pl.pallas_call(
+        functools.partial(norm_kernel, pre.shape[1] * PAIR * PAIR),
+        out_shape=jax.ShapeDtypeStruct(pre.shape, jnp.bfloat16),
+        in_specs=[VMEM] * 6,
+        out_specs=VMEM,
+        compiler_params=PARAMS,
+        name="finish",
+    )(pre, *stats, gain.reshape(1, -1))
+
+
+def three_terms(gain):
+    first = lax.reduce_precision(gain, 8, 7)
+    left = gain - first
+    second = lax.reduce_precision(left, 8, 7)
+    third = left - second
+    return jnp.stack([first, second, third]).astype(jnp.bfloat16)
+
+
+def planned(*arrays):
+    return planned_steps(*arrays)
+
+
+def planned_steps(
+    queries,
+    latents,
+    rope_key,
+    w_key,
+    w_value,
+    w_out,
+    resid,
+    gain_mix,
+    w_gate,
+    w_up,
+    w_down,
+    gain_out,
+):
+    _, p, _, c = coordinates()
+    local_rows = queries.shape[0]
+    positions = lax.axis_index("sp") * local_rows + jnp.arange(local_rows, dtype=jnp.int32)
+    cosine, sine = rotary_tables(positions, ROPE, GRID_W)
+    key_rot = rotate(rope_key, cosine, sine)
+
+    half = local_rows // PAIR
+    wide = jnp.concatenate(
+        [latents, key_rot, jnp.zeros((local_rows, LANES - ROPE), jnp.bfloat16)], axis=1
+    )
+    piece = lax.dynamic_slice_in_dim(wide, c * half, half, 0)
+    near = flip(piece, dp=1)
+    far = flip(piece, dr=2, dp=1)
+    cut = half // 2
+    across_low = flip(far[:cut], dp=1)
+    across_high = flip(near[cut:], dr=2, dp=1)
+    crossed = flip(piece, dr=1)
+    first = jnp.concatenate([near, far], axis=0)
+    first = [piece, first, crossed, flip(first, dr=1)]
+    last = jnp.concatenate([across_low, across_high], axis=0)
+    last = [last, flip(last, dr=1)]
+    first = jnp.concatenate(first, axis=0)
+    first = [first, partner(first)]
+    last = jnp.concatenate(last, axis=0)
+    last = [last, partner(last)]
+    blocks = first + last
+
+    shards = {"g": w_gate, "u": w_up, "d": w_down}
+    swapped = {}
+    for name, shard in shards.items():
+        swapped[name] = exchange_halves(shard)
+
+    heads_own = attend(queries, cosine, sine, blocks, w_key, w_value)
+    swapped["d"], heads_own = lax.optimization_barrier((swapped["d"], heads_own))
+    gathered = []
+    for name, shard in shards.items():
+        shard = jnp.where(p == c, shard, swapped[name])
+        w_near = flip(shard, dr=1)
+        w_far = flip(shard, dr=2)
+        w_across = flip(w_far, dr=1)
+        gathered.append([shard, w_near, w_far, w_across])
+
+
+    gains = jnp.pad(three_terms(gain_mix), ((0, 13), (0, 0)))
+    resid_own = jnp.concatenate([resid, gains], axis=0)
+    resid_pieces = []
+    for dy, k in ROUNDS:
+        resid_pieces.append(spread(resid_own, dy, k))
+    out_other = flip(w_out, dy=1)
+    w_partner = partner(w_out)
+    out_last = partner(out_other)
+    w_pieces = [w_out, w_partner, out_other, out_last]
+    heads = []
+    for dy, k in ROUNDS:
+        heads.append(spread(heads_own, dy, k))
+    hidden = mix(heads, w_pieces, resid_pieces)
+    got = partner(hidden)
+    sums = feed_up(hidden, got, gathered[0], gathered[1])
+    sums_got = partner(sums)
+    terms = list(feed_down(sums, sums_got, gathered[2]))
+    for at, (dy, dp) in enumerate(ROUNDS):
+        if dy or dp:
+            terms[at] = flip(terms[at], dp=dp, dy=dy)
+    pre, stats = add_up(hidden, got, terms)
+    stat_y = flip(stats, dy=1)
+    stat_yc = flip(stats, dy=1, dc=1)
+    stat_c = partner(stats)
+    return finish(pre, [stats, stat_c, stat_y, stat_yc], gain_out)
 
 
 def solution(mesh):
@@ -183,6 +757,7 @@
         P("tp", "sp"),
         P("tp"),
     )
+    body = planned if fits_plan(mesh) else local
     return jax.shard_map(
-        local, mesh=mesh, in_specs=placed, out_specs=P("sp", "tp"), check_vma=False
-    )
+        body, mesh=mesh, in_specs=placed, out_specs=P("sp", "tp"), check_vma=False
+    )

time: 325 us -> 171 us (0.53)
  waiting for transfers between devices: 190 us -> 84.9 us
  blocking collectives: 90.5 us -> 0 us
  starting transfers between devices: 0.21 us -> 51.2 us
  Pallas kernels: 0 us -> 23.5 us
  matrix products: 19.2 us -> 0 us
  between operations: 14.9 us -> 0.41 us
  local copies, waits for them, and re-layouts: 2.7 us -> 7.74 us
  other arithmetic: 6.87 us -> 3.15 us
    all_gather x4 -> x0, waiting for transfers between devices: 144 us -> none  [the longest x1 63.1 us: local(): lax.all_gather(w_down, 'sp', axis=1, tiled=True)]
    ppermute x0 -> x40, waiting for transfers between devices: none -> 84.9 us  [move(): return lax.ppermute(array, BOTH, pairs)]
    all_gather x4 -> x0, blocking collectives: 79 us -> none  [the longest x1 34.8 us: local(): lax.all_gather(latent_part, 'sp', axis=0, tiled=True)]
    ppermute x0 -> x40, starting transfers between devices: none -> 51.2 us  [move(): return lax.ppermute(array, BOTH, pairs)]
    reduce_scatter x2 -> x0, waiting for transfers between devices: 44.1 us -> none  [the longest x1 22.5 us: local(): lax.psum_scatter(projected.astype(jnp.bfloat16), 'tp', scatter_dimension=...]
    pallas_call x0 -> x6, Pallas kernels: none -> 23.5 us  [the longest x1 8.04 us: mix(): pl.pallas_call(mix_kernel, out_shape=jax.ShapeDtypeStruct((rows, width_to...]
    dot_general x8 -> x0, matrix products: 19.2 us -> none  [the longest x1 5.41 us: local(): jnp.dot(hidden, lax.all_gather(w_down, 'sp', axis=1, tiled=True), preferr...]
    psum x2 -> x0, blocking collectives: 11.5 us -> none  [split_norm(): lax.psum((jnp.sum(rows_in, axis=1), jnp.sum(rows_in * rows_in, axis=1)),...]
  transfers between devices with their start and end apart: 6 -> 40, of which waited for: 5 -> 16; matrix products, arithmetic and copies ran while one was open for 3% -> 4% of each run, Pallas kernels for 0% -> 8%
where the time goes in v1:
time: 171 us
  waiting for transfers between devices  84.9 us (50%)
  starting transfers between devices  51.2 us (30%)
  Pallas kernels  23.5 us (14%)
  local copies, waits for them, and re-layouts  7.74 us (5%)
  other arithmetic  3.15 us (2%)
    ppermute x40, waiting for transfers between devices, move(): return lax.ppermute(array, BOTH, pairs)  84.9 us
    ppermute x40, starting transfers between devices, move(): return lax.ppermute(array, BOTH, pairs)  51.2 us
    pallas_call x1, Pallas kernels, mix(): pl.pallas_call(mix_kernel, out_shape=jax.ShapeDtypeStruct((rows, width_to...  8.04 us
    pallas_call x1, Pallas kernels, attend(): pl.pallas_call(functools.partial(attention_kernel, (NOPE + ROPE) ** (-0.5...  5.7 us
    unnamed x39, local copies, waits for them, and re-layouts  4.78 us
    pallas_call x1, Pallas kernels, feed_up(): pl.pallas_call(up_kernel, out_shape=jax.ShapeDtypeStruct((PAIR * rows, 2...  3.84 us
    pallas_call x1, Pallas kernels, feed_down(): pl.pallas_call(down_kernel, out_shape=(block,) * 4, in_specs=[HBM] * 6, o...  3.51 us
  transfers between devices with their start and end apart: 40, of which 16 were waited for; matrix products, arithmetic and copies ran while one was open for 4% of the time, Pallas kernels for 8%

profile of v1, /device:TPU:0, one launch (start us, length us, event | category | flops | bytes accessed | tf_op | source)
XLA Modules:
  0.0 170.9 jit_solution(6454207240268769728)
XLA Ops:
  0.7 0.7 fusion.18
  1.8 0.7 constant_dynamic-update-slice_fusion.4
  2.6 5.1 %collective-permute-start.2 = (bf16[96,640]{1,0:T(8,128)(2,1)S(1)}, bf16[96,640]{1,0:T(8,128)(2,1)S(1)}, u32[]{:S(2)}, u32[]{:S(2)}) collective-permute-start(bf16[96,640]{1,0:T(8,128)(2,1)S(1)} %get-tuple-element.22), channel_id=1, source_target_pairs={{0,24},{1,25},{2,26},{3,27},{8,16},{9,17},{10,18},{11,19},{4,28},{... | collective-permute-start | bytes 368648 | tf_op jit(solution)/shard_map/ppermute | solution.py:206
  7.7 1.5 collective-permute-start.3
  9.2 1.5 collective-permute-start.15
  10.8 0.8 collective-permute-start.17
  11.9 3.1 %collective-permute-start.18 = (bf16[208,512]{1,0:T(8,128)(2,1)S(1)}, bf16[208,512]{1,0:T(8,128)(2,1)S(1)}, u32[]{:S(2)}, u32[]{:S(2)}) collective-permute-start(bf16[208,512]{1,0:T(8,128)(2,1)S(1)} %pad_maximum_fusion.1), channel_id=1, source_target_pairs={{0,8},{1,0},{2,10},{3,2},{8,9},{9,1},{10,11},{11,3},{4,12},{5,4},{... | collective-permute-start | bytes 638984 | tf_op jit(solution)/shard_map/ppermute | solution.py:206
  16.9 1.4 collective-permute-start.6
  19.0 4.1 %collective-permute-done.4 = bf16[192,640]{1,0:T(8,128)(2,1)S(1)} collective-permute-done((bf16[192,640]{1,0:T(8,128)(2,1)S(1)}, bf16[192,640]{1,0:T(8,128)(2,1)S(1)}, u32[]{:S(2)}, u32[]{:S(2)}) %collective-permute-start.4) | collective-permute-done | bytes 245792 | tf_op jit(solution)/shard_map/ppermute | solution.py:206
  23.7 0.7 constant_dynamic-update-slice_fusion.refs_3_
  24.4 4.7 %collective-permute-done.7 = bf16[48,640]{1,0:T(8,128)(2,1)S(1)} collective-permute-done((bf16[48,640]{1,0:T(8,128)(2,1)S(1)}, bf16[48,640]{1,0:T(8,128)(2,1)S(1)}, u32[]{:S(2)}, u32[]{:S(2)}) %collective-permute-start.7) | collective-permute-done | bytes 61472 | tf_op jit(solution)/shard_map/ppermute | solution.py:206
  31.1 3.8 %collective-permute-done.8 = bf16[96,640]{1,0:T(8,128)(2,1)S(1)} collective-permute-done((bf16[96,640]{1,0:T(8,128)(2,1)S(1)}, bf16[96,640]{1,0:T(8,128)(2,1)S(1)}, u32[]{:S(2)}, u32[]{:S(2)}) %collective-permute-start.8) | collective-permute-done | bytes 122912 | tf_op jit(solution)/shard_map/ppermute | solution.py:206
  35.6 1.3 collective-permute-start.16
  38.9 0.8 collective-permute-start.9
  39.8 0.8 copy-done.12
  40.5 1.4 collective-permute-start.26
  42.6 6.8 %collective-permute-start.20 = (bf16[208,512]{1,0:T(8,128)(2,1)}, bf16[208,512]{1,0:T(8,128)(2,1)S(1)}, u32[]{:S(2)}, u32[]{:S(2)}) collective-permute-start(bf16[208,512]{1,0:T(8,128)(2,1)} %copy-done.13), channel_id=1, source_target_pairs={{0,10},{1,2},{2,8},{3,0},{8,11},{9,3},{10,9},{11,1},{4,14},{5,6},{... | collective-permute-start | bytes 638984 | tf_op jit(solution)/shard_map/ppermute | solution.py:206
  49.4 1.0 broadcast_select_fusion.2.refs_0_
  50.5 5.7 %attend.1 = bf16[192,256]{1,0:T(8,128)(2,1)S(1)} custom-call(bf16[192,384]{1,0:T(8,128)(2,1)S(1)} %copy-done.5, f32[192,16]{1,0:T(8,128)S(1)} %copy.24.refs_1_, f32[192,16]{1,0:T(8,128)S(1)} %sin.3.refs_2_, bf16[576,640]{1,0:T(8,128)(2,1)} %constant_dynamic-update-slice_fusion.refs_3_, bf16[576,640]{1,0:T(8,128)(2,1)} %collective-permute-done.5.refs_4_, ...), custom_call_target="tpu_custom_call" | custom-call | tf_op jit(solution)/shard_map/attend/pallas_call | solution.py:335
  56.2 0.8 collective-permute-start.10
  57.0 5.2 %collective-permute-start.11 = (bf16[192,256]{1,0:T(8,128)(2,1)S(1)}, bf16[192,256]{1,0:T(8,128)(2,1)S(1)}, u32[]{:S(2)}, u32[]{:S(2)}) collective-permute-start(bf16[192,256]{1,0:T(8,128)(2,1)S(1)} %attend.1), channel_id=1, source_target_pairs={{0,8},{1,0},{2,10},{3,2},{8,9},{9,1},{10,11},{11,3},{4,12},{5,4},{... | collective-permute-start | bytes 294920 | tf_op jit(solution)/shard_map/ppermute | solution.py:206
  62.3 1.4 collective-permute-start.12
  63.7 1.0 broadcast_select_fusion.1.refs_4_
  64.7 1.0 collective-permute-start.24
  65.8 2.0 %collective-permute-start.28 = (bf16[256,768]{1,0:T(8,128)(2,1)S(1)}, bf16[256,768]{1,0:T(8,128)(2,1)S(1)}, u32[]{:S(2)}, u32[]{:S(2)}) collective-permute-start(bf16[256,768]{1,0:T(8,128)(2,1)S(1)} %broadcast_select_fusion.1.refs_4_), channel_id=1, source_target_pairs={{0,16},{1,17},{2,18},{3,19},{8,24},{9,25},{10,26},{11,27},{4,20},{... | collective-permute-start | bytes 1179656 | tf_op jit(solution)/shard_map/ppermute | solution.py:206
  67.7 1.8 %collective-permute-done.12.refs_2_ = bf16[192,256]{1,0:T(8,128)(2,1)S(1)} collective-permute-done((bf16[192,256]{1,0:T(8,128)(2,1)S(1)}, bf16[192,256]{1,0:T(8,128)(2,1)S(1)}, u32[]{:S(2)}, u32[]{:S(2)}) %collective-permute-start.12) | collective-permute-done | bytes 98336 | tf_op jit(solution)/shard_map/ppermute | solution.py:206
  70.0 8.0 %mix.1.own_ref = bf16[192,2048]{1,0:T(8,128)(2,1)S(1)} custom-call(bf16[192,256]{1,0:T(8,128)(2,1)S(1)} %collective-permute-done.10.refs_0_, bf16[192,256]{1,0:T(8,128)(2,1)S(1)} %collective-permute-done.11.refs_1_, bf16[192,256]{1,0:T(8,128)(2,1)S(1)} %collective-permute-done.12.refs_2_, bf16[192,256]{1,0:T(8,128)(2,1)S(1)} %collective-permute-done.13.refs_3_, ...), custom_call_target="tpu_custom_call" | custom-call | tf_op jit(solution)/shard_map/mix/pallas_call | solution.py:407
  78.2 1.4 collective-permute-start.23
  80.3 13.8 %collective-permute-done.24.refs_2_ = bf16[256,768]{1,0:T(8,128)(2,1)S(1)} collective-permute-done((bf16[256,768]{1,0:T(8,128)(2,1)S(1)}, bf16[256,768]{1,0:T(8,128)(2,1)S(1)}, u32[]{:S(2)}, u32[]{:S(2)}) %collective-permute-start.24) | collective-permute-done | bytes 393248 | tf_op jit(solution)/shard_map/ppermute | solution.py:206
  94.1 1.4 collective-permute-start.25
  95.6 7.0 %collective-permute-done.28.refs_6_ = bf16[256,768]{1,0:T(8,128)(2,1)S(1)} collective-permute-done((bf16[256,768]{1,0:T(8,128)(2,1)S(1)}, bf16[256,768]{1,0:T(8,128)(2,1)S(1)}, u32[]{:S(2)}, u32[]{:S(2)}) %collective-permute-start.28) | collective-permute-done | bytes 393248 | tf_op jit(solution)/shard_map/ppermute | solution.py:206
  102.5 1.4 collective-permute-start.29
  104.0 3.1 %collective-permute-done.25.refs_3_ = bf16[256,768]{1,0:T(8,128)(2,1)S(1)} collective-permute-done((bf16[256,768]{1,0:T(8,128)(2,1)S(1)}, bf16[256,768]{1,0:T(8,128)(2,1)S(1)}, u32[]{:S(2)}, u32[]{:S(2)}) %collective-permute-start.25) | collective-permute-done | bytes 393248 | tf_op jit(solution)/shard_map/ppermute | solution.py:206
  107.1 7.9 %collective-permute-done.29.refs_7_ = bf16[256,768]{1,0:T(8,128)(2,1)S(1)} collective-permute-done((bf16[256,768]{1,0:T(8,128)(2,1)S(1)}, bf16[256,768]{1,0:T(8,128)(2,1)S(1)}, u32[]{:S(2)}, u32[]{:S(2)}) %collective-permute-start.29) | collective-permute-done | bytes 393248 | tf_op jit(solution)/shard_map/ppermute | solution.py:206
  115.0 3.8 %feed_up.1.own_ref = bf16[384,1536]{1,0:T(8,128)(2,1)S(1)} custom-call(bf16[192,2048]{1,0:T(8,128)(2,1)S(1)} %mix.1.own_ref, bf16[192,2048]{1,0:T(8,128)(2,1)S(1)} %collective-permute-done.21.got_ref, bf16[256,768]{1,0:T(8,128)(2,1)S(1)} %broadcast_select_fusion.2.refs_0_, bf16[256,768]{1,0:T(8,128)(2,1)S(1)} %collective-permute-done.23.refs_1_, ...), custom_call_target="tpu_custom_call" | custom-call | tf_op jit(solution)/shard_map/feed_up/pallas_call | solution.py:488
  119.2 1.3 collective-permute-start.31
  120.5 18.3 %collective-permute-done.32.refs_2_ = bf16[768,256]{1,0:T(8,128)(2,1)S(1)} collective-permute-done((bf16[768,256]{1,0:T(8,128)(2,1)S(1)}, bf16[768,256]{1,0:T(8,128)(2,1)S(1)}, u32[]{:S(2)}, u32[]{:S(2)}) %collective-permute-start.32) | collective-permute-done | bytes 393248 | tf_op jit(solution)/shard_map/ppermute | solution.py:206
  138.8 1.2 collective-permute-start.33
  140.0 9.9 %collective-permute-done.33.refs_3_ = bf16[768,256]{1,0:T(8,128)(2,1)S(1)} collective-permute-done((bf16[768,256]{1,0:T(8,128)(2,1)S(1)}, bf16[768,256]{1,0:T(8,128)(2,1)S(1)}, u32[]{:S(2)}, u32[]{:S(2)}) %collective-permute-start.33) | collective-permute-done | bytes 393248 | tf_op jit(solution)/shard_map/ppermute | solution.py:206
  149.9 3.5 %feed_down.1 = (bf16[192,512]{1,0:T(8,128)(2,1)S(1)}, bf16[192,512]{1,0:T(8,128)(2,1)S(1)}, bf16[192,512]{1,0:T(8,128)(2,1)S(1)}, bf16[192,512]{1,0:T(8,128)(2,1)S(1)}) custom-call(bf16[384,1536]{1,0:T(8,128)(2,1)S(1)} %feed_up.1.own_ref, bf16[384,1536]{1,0:T(8,128)(2,1)S(1)} %collective-permute-done.30.got_ref, ...), custom_call_target="tpu_custom_call" | custom-call | tf_op jit(solution)/shard_map/feed_down/pallas_call | solution.py:557
  153.5 1.5 collective-permute-start.35
  155.0 1.9 %collective-permute-start.36 = (bf16[192,512]{1,0:T(8,128)(2,1)S(1)}, bf16[192,512]{1,0:T(8,128)(2,1)S(1)}, u32[]{:S(2)}, u32[]{:S(2)}) collective-permute-start(bf16[192,512]{1,0:T(8,128)(2,1)S(1)} %get-tuple-element.18), channel_id=1, source_target_pairs={{0,10},{1,11},{2,8},{3,9},{8,2},{9,3},{10,0},{11,1},{4,14},{5,15},... | collective-permute-start | bytes 589832 | tf_op jit(solution)/shard_map/ppermute | solution.py:206
  157.0 4.3 %collective-permute-done.34.refs_1_ = bf16[192,512]{1,0:T(8,128)(2,1)S(1)} collective-permute-done((bf16[192,512]{1,0:T(8,128)(2,1)S(1)}, bf16[192,512]{1,0:T(8,128)(2,1)S(1)}, u32[]{:S(2)}, u32[]{:S(2)}) %collective-permute-start.34) | collective-permute-done | bytes 196640 | tf_op jit(solution)/shard_map/ppermute | solution.py:206
  161.3 3.4 %collective-permute-done.36.refs_3_ = bf16[192,512]{1,0:T(8,128)(2,1)S(1)} collective-permute-done((bf16[192,512]{1,0:T(8,128)(2,1)S(1)}, bf16[192,512]{1,0:T(8,128)(2,1)S(1)}, u32[]{:S(2)}, u32[]{:S(2)}) %collective-permute-start.36) | collective-permute-done | bytes 196640 | tf_op jit(solution)/shard_map/ppermute | solution.py:206
  164.6 1.4 add_up.1
  166.8 1.1 collective-permute-start.39
  168.0 1.9 %collective-permute-done.38.c_ref = f32[8,192]{1,0:T(8,128)S(1)} collective-permute-done((f32[8,192]{1,0:T(8,128)S(1)}, f32[8,192]{1,0:T(8,128)S(1)}, u32[]{:S(2)}, u32[]{:S(2)}) %collective-permute-start.38) | collective-permute-done | bytes 6176 | tf_op jit(solution)/shard_map/ppermute | solution.py:206
  169.9 1.0 finish.1
  (106 shorter events, 12.5 us)
Async XLA Ops:
  0.0 10.7 %copy-start.16 = (f32[512]{0:T(512)S(1)}, f32[512]{0:T(512)}, u32[]{:S(2)}) copy-start(f32[512]{0:T(512)} %param.19) | copy-start | bytes 6148
  0.0 10.7 %copy-start.15 = (bf16[192,512]{1,0:T(8,128)(2,1)S(1)}, bf16[192,512]{1,0:T(8,128)(2,1)}, u32[]{:S(2)}) copy-start(bf16[192,512]{1,0:T(8,128)(2,1)} %param.18) | copy-start | bytes 589828
  2.6 9.3 %collective-permute-start.2 = (bf16[96,640]{1,0:T(8,128)(2,1)S(1)}, bf16[96,640]{1,0:T(8,128)(2,1)S(1)}, u32[]{:S(2)}, u32[]{:S(2)}) collective-permute-start(bf16[96,640]{1,0:T(8,128)(2,1)S(1)} %get-tuple-element.22), channel_id=1, source_target_pairs={{0,24},{1,25},{2,26},{3,27},{8,16},{9,17},{10,18},{11,19},{4,28},{... | collective-permute-start | bytes 368648 | tf_op jit(solution)/shard_map/ppermute | solution.py:206
  7.7 7.3 %collective-permute-start.1 = (bf16[96,640]{1,0:T(8,128)(2,1)S(1)}, bf16[96,640]{1,0:T(8,128)(2,1)S(1)}, u32[]{:S(2)}, u32[]{:S(2)}) collective-permute-start(bf16[96,640]{1,0:T(8,128)(2,1)S(1)} %get-tuple-element.22), channel_id=1, source_target_pairs={{0,8},{1,9},{2,10},{3,11},{8,0},{9,1},{10,2},{11,3},{4,12},{5,13},... | collective-permute-start | bytes 368648 | tf_op jit(solution)/shard_map/ppermute | solution.py:206
  7.7 9.3 %collective-permute-start.3 = (bf16[96,640]{1,0:T(8,128)(2,1)S(1)}, bf16[96,640]{1,0:T(8,128)(2,1)S(1)}, u32[]{:S(2)}, u32[]{:S(2)}) collective-permute-start(bf16[96,640]{1,0:T(8,128)(2,1)S(1)} %get-tuple-element.22), channel_id=1, source_target_pairs={{0,4},{1,5},{2,6},{3,7},{8,12},{9,13},{10,14},{11,15},{4,0},{5,1},... | collective-permute-start | bytes 368648 | tf_op jit(solution)/shard_map/ppermute | solution.py:206
  9.2 26.5 %collective-permute-start.15 = (bf16[256,2048]{1,0:T(8,128)(2,1)S(1)}, bf16[256,2048]{1,0:T(8,128)(2,1)S(1)}, u32[]{:S(2)}, u32[]{:S(2)}) collective-permute-start(bf16[256,2048]{1,0:T(8,128)(2,1)S(1)} %copy-done), channel_id=1, source_target_pairs={{0,2},{1,3},{2,0},{3,1},{8,10},{9,11},{10,8},{11,9},{4,6},{5,7},{6... | collective-permute-start | bytes 3145736 | tf_op jit(solution)/shard_map/ppermute | solution.py:206
  10.8 27.5 %copy-start.13 = (bf16[208,512]{1,0:T(8,128)(2,1)}, bf16[208,512]{1,0:T(8,128)(2,1)S(1)}, u32[]{:S(2)}) copy-start(bf16[208,512]{1,0:T(8,128)(2,1)S(1)} %pad_maximum_fusion.1) | copy-start | bytes 638980
  10.8 19.6 %copy-start.8 = (bf16[768,256]{1,0:T(8,128)(2,1)S(1)}, bf16[768,256]{1,0:T(8,128)(2,1)}, u32[]{:S(2)}) copy-start(bf16[768,256]{1,0:T(8,128)(2,1)} %param.22) | copy-start | bytes 1179652
  10.8 24.1 %copy-start.7 = (bf16[256,768]{1,0:T(8,128)(2,1)S(1)}, bf16[256,768]{1,0:T(8,128)(2,1)}, u32[]{:S(2)}) copy-start(bf16[256,768]{1,0:T(8,128)(2,1)} %param.20) | copy-start | bytes 1179652
  10.8 18.3 %collective-permute-start.17 = (bf16[208,512]{1,0:T(8,128)(2,1)S(1)}, bf16[208,512]{1,0:T(8,128)(2,1)S(1)}, u32[]{:S(2)}, u32[]{:S(2)}) collective-permute-start(bf16[208,512]{1,0:T(8,128)(2,1)S(1)} %pad_maximum_fusion.1), channel_id=1, source_target_pairs={{0,0},{1,8},{2,2},{3,10},{8,1},{9,9},{10,3},{11,11},{4,4},{5,12},{... | collective-permute-start | bytes 638984 | tf_op jit(solution)/shard_map/ppermute | solution.py:206
  11.9 17.8 %collective-permute-start.18 = (bf16[208,512]{1,0:T(8,128)(2,1)S(1)}, bf16[208,512]{1,0:T(8,128)(2,1)S(1)}, u32[]{:S(2)}, u32[]{:S(2)}) collective-permute-start(bf16[208,512]{1,0:T(8,128)(2,1)S(1)} %pad_maximum_fusion.1), channel_id=1, source_target_pairs={{0,8},{1,0},{2,10},{3,2},{8,9},{9,1},{10,11},{11,3},{4,12},{5,4},{... | collective-permute-start | bytes 638984 | tf_op jit(solution)/shard_map/ppermute | solution.py:206
  15.0 8.1 %collective-permute-start.4 = (bf16[192,640]{1,0:T(8,128)(2,1)S(1)}, bf16[192,640]{1,0:T(8,128)(2,1)S(1)}, u32[]{:S(2)}, u32[]{:S(2)}) collective-permute-start(bf16[192,640]{1,0:T(8,128)(2,1)S(1)} %pad_maximum_fusion), channel_id=1, source_target_pairs={{0,4},{1,5},{2,6},{3,7},{8,12},{9,13},{10,14},{11,15},{4,0},{5,1},... | collective-permute-start | bytes 737288 | tf_op jit(solution)/shard_map/ppermute | solution.py:206
  16.9 7.4 %collective-permute-start.6 = (bf16[48,640]{1,0:T(8,128)(2,1)S(1)}, bf16[48,640]{1,0:T(8,128)(2,1)S(1)}, u32[]{:S(2)}, u32[]{:S(2)}) collective-permute-start(bf16[48,640]{1,0:T(8,128)(2,1)S(1)} %slice.16), channel_id=1, source_target_pairs={{0,8},{1,9},{2,10},{3,11},{8,0},{9,1},{10,2},{11,3},{4,12},{5,13},... | collective-permute-start | bytes 184328 | tf_op jit(solution)/shard_map/ppermute | solution.py:206
  23.1 6.1 %collective-permute-start.7 = (bf16[48,640]{1,0:T(8,128)(2,1)S(1)}, bf16[48,640]{1,0:T(8,128)(2,1)S(1)}, u32[]{:S(2)}, u32[]{:S(2)}) collective-permute-start(bf16[48,640]{1,0:T(8,128)(2,1)S(1)} %slice.17), channel_id=1, source_target_pairs={{0,24},{1,25},{2,26},{3,27},{8,16},{9,17},{10,18},{11,19},{4,28},{... | collective-permute-start | bytes 184328 | tf_op jit(solution)/shard_map/ppermute | solution.py:206
  24.4 39.3 %collective-permute-start.14 = (bf16[256,2048]{1,0:T(8,128)(2,1)S(1)}, bf16[256,2048]{1,0:T(8,128)(2,1)S(1)}, u32[]{:S(2)}, u32[]{:S(2)}) collective-permute-start(bf16[256,2048]{1,0:T(8,128)(2,1)S(1)} %copy-done), channel_id=1, source_target_pairs={{0,1},{1,0},{2,3},{3,2},{8,9},{9,8},{10,11},{11,10},{4,5},{5,4},{6... | collective-permute-start | bytes 3145736 | tf_op jit(solution)/shard_map/ppermute | solution.py:206
  29.1 13.5 %collective-permute-start.5 = (bf16[576,640]{1,0:T(8,128)(2,1)}, bf16[576,640]{1,0:T(8,128)(2,1)}, u32[]{:S(2)}, u32[]{:S(2)}) collective-permute-start(bf16[576,640]{1,0:T(8,128)(2,1)} %constant_dynamic-update-slice_fusion.refs_3_), channel_id=1, source_target_pairs={{0,1},{1,0},{2,3},{3,2},{8,9},{9,8},{10,11},{11,10},{4,5},{5,4},{6... | collective-permute-start | bytes 2211848 | tf_op jit(solution)/shard_map/ppermute | solution.py:206
  29.1 5.8 %collective-permute-start.8 = (bf16[96,640]{1,0:T(8,128)(2,1)S(1)}, bf16[96,640]{1,0:T(8,128)(2,1)S(1)}, u32[]{:S(2)}, u32[]{:S(2)}) collective-permute-start(bf16[96,640]{1,0:T(8,128)(2,1)S(1)} %pad_maximum_fusion.2), channel_id=1, source_target_pairs={{0,4},{1,5},{2,6},{3,7},{8,12},{9,13},{10,14},{11,15},{4,0},{5,1},... | collective-permute-start | bytes 368648 | tf_op jit(solution)/shard_map/ppermute | solution.py:206
  30.4 8.5 %collective-permute-start = (bf16[768,256]{1,0:T(8,128)(2,1)S(1)}, bf16[768,256]{1,0:T(8,128)(2,1)S(1)}, u32[]{:S(2)}, u32[]{:S(2)}) collective-permute-start(bf16[768,256]{1,0:T(8,128)(2,1)S(1)} %copy-done.8), channel_id=1, source_target_pairs={{1,8},{3,10},{8,1},{10,3},{5,12},{7,14},{12,5},{14,7},{17,24},{19,... | collective-permute-start | bytes 1179656 | tf_op jit(solution)/shard_map/ppermute | solution.py:206
  34.9 4.8 %collective-permute-start.22 = (bf16[256,768]{1,0:T(8,128)(2,1)S(1)}, bf16[256,768]{1,0:T(8,128)(2,1)S(1)}, u32[]{:S(2)}, u32[]{:S(2)}) collective-permute-start(bf16[256,768]{1,0:T(8,128)(2,1)S(1)} %copy-done.7), channel_id=1, source_target_pairs={{1,8},{3,10},{8,1},{10,3},{5,12},{7,14},{12,5},{14,7},{17,24},{19,... | collective-permute-start | bytes 1179656 | tf_op jit(solution)/shard_map/ppermute | solution.py:206
  35.6 34.4 %collective-permute-start.16 = (bf16[256,2048]{1,0:T(8,128)(2,1)S(1)}, bf16[256,2048]{1,0:T(8,128)(2,1)}, u32[]{:S(2)}, u32[]{:S(2)}) collective-permute-start(bf16[256,2048]{1,0:T(8,128)(2,1)S(1)} %collective-permute-done.15.refs_6_), channel_id=1, source_target_pairs={{0,1},{1,0},{2,3},{3,2},{8,9},{9,8},{10,11},{11,10},{4,5},{5,4},{6... | collective-permute-start | bytes 3145736 | tf_op jit(solution)/shard_map/ppermute | solution.py:206
  38.9 3.0 %collective-permute-start.9 = (bf16[192,640]{1,0:T(8,128)(2,1)}, bf16[192,640]{1,0:T(8,128)(2,1)}, u32[]{:S(2)}, u32[]{:S(2)}) collective-permute-start(bf16[192,640]{1,0:T(8,128)(2,1)} %constant_dynamic-update-slice_fusion.5.refs_5_), channel_id=1, source_target_pairs={{0,1},{1,0},{2,3},{3,2},{8,9},{9,8},{10,11},{11,10},{4,5},{5,4},{6... | collective-permute-start | bytes 737288 | tf_op jit(solution)/shard_map/ppermute | solution.py:206
  40.5 21.8 %collective-permute-start.26 = (bf16[256,768]{1,0:T(8,128)(2,1)}, bf16[256,768]{1,0:T(8,128)(2,1)}, u32[]{:S(2)}, u32[]{:S(2)}) collective-permute-start(bf16[256,768]{1,0:T(8,128)(2,1)} %param.21), channel_id=1, source_target_pairs={{1,8},{3,10},{8,1},{10,3},{5,12},{7,14},{12,5},{14,7},{17,24},{19,... | collective-permute-start | bytes 1179656 | tf_op jit(solution)/shard_map/ppermute | solution.py:206
  41.9 14.3 %collective-permute-start.19 = (bf16[208,512]{1,0:T(8,128)(2,1)}, bf16[208,512]{1,0:T(8,128)(2,1)S(1)}, u32[]{:S(2)}, u32[]{:S(2)}) collective-permute-start(bf16[208,512]{1,0:T(8,128)(2,1)} %copy-done.13), channel_id=1, source_target_pairs={{0,2},{1,10},{2,0},{3,8},{8,3},{9,11},{10,1},{11,9},{4,6},{5,14},{... | collective-permute-start | bytes 638984 | tf_op jit(solution)/shard_map/ppermute | solution.py:206
  42.6 14.4 %collective-permute-start.20 = (bf16[208,512]{1,0:T(8,128)(2,1)}, bf16[208,512]{1,0:T(8,128)(2,1)S(1)}, u32[]{:S(2)}, u32[]{:S(2)}) collective-permute-start(bf16[208,512]{1,0:T(8,128)(2,1)} %copy-done.13), channel_id=1, source_target_pairs={{0,10},{1,2},{2,8},{3,0},{8,11},{9,3},{10,9},{11,1},{4,14},{5,6},{... | collective-permute-start | bytes 638984 | tf_op jit(solution)/shard_map/ppermute | solution.py:206
  56.2 13.8 %copy-start.4 = (bf16[208,512]{1,0:T(8,128)(2,1)S(1)}, bf16[208,512]{1,0:T(8,128)(2,1)}, u32[]{:S(2)}) copy-start(bf16[208,512]{1,0:T(8,128)(2,1)} %copy-done.3) | copy-start | bytes 638980
  56.2 8.5 %collective-permute-start.10 = (bf16[192,256]{1,0:T(8,128)(2,1)S(1)}, bf16[192,256]{1,0:T(8,128)(2,1)S(1)}, u32[]{:S(2)}, u32[]{:S(2)}) collective-permute-start(bf16[192,256]{1,0:T(8,128)(2,1)S(1)} %attend.1), channel_id=1, source_target_pairs={{0,0},{1,8},{2,2},{3,10},{8,1},{9,9},{10,3},{11,11},{4,4},{5,12},{... | collective-permute-start | bytes 294920 | tf_op jit(solution)/shard_map/ppermute | solution.py:206
  57.0 8.7 %collective-permute-start.11 = (bf16[192,256]{1,0:T(8,128)(2,1)S(1)}, bf16[192,256]{1,0:T(8,128)(2,1)S(1)}, u32[]{:S(2)}, u32[]{:S(2)}) collective-permute-start(bf16[192,256]{1,0:T(8,128)(2,1)S(1)} %attend.1), channel_id=1, source_target_pairs={{0,8},{1,0},{2,10},{3,2},{8,9},{9,1},{10,11},{11,3},{4,12},{5,4},{... | collective-permute-start | bytes 294920 | tf_op jit(solution)/shard_map/ppermute | solution.py:206
  62.3 7.2 %collective-permute-start.12 = (bf16[192,256]{1,0:T(8,128)(2,1)S(1)}, bf16[192,256]{1,0:T(8,128)(2,1)S(1)}, u32[]{:S(2)}, u32[]{:S(2)}) collective-permute-start(bf16[192,256]{1,0:T(8,128)(2,1)S(1)} %attend.1), channel_id=1, source_target_pairs={{0,2},{1,10},{2,0},{3,8},{8,3},{9,11},{10,1},{11,9},{4,6},{5,14},{... | collective-permute-start | bytes 294920 | tf_op jit(solution)/shard_map/ppermute | solution.py:206
  63.7 6.4 %collective-permute-start.13 = (bf16[192,256]{1,0:T(8,128)(2,1)S(1)}, bf16[192,256]{1,0:T(8,128)(2,1)S(1)}, u32[]{:S(2)}, u32[]{:S(2)}) collective-permute-start(bf16[192,256]{1,0:T(8,128)(2,1)S(1)} %attend.1), channel_id=1, source_target_pairs={{0,10},{1,2},{2,8},{3,0},{8,11},{9,3},{10,9},{11,1},{4,14},{5,6},{... | collective-permute-start | bytes 294920 | tf_op jit(solution)/shard_map/ppermute | solution.py:206
  64.7 29.4 %collective-permute-start.24 = (bf16[256,768]{1,0:T(8,128)(2,1)S(1)}, bf16[256,768]{1,0:T(8,128)(2,1)S(1)}, u32[]{:S(2)}, u32[]{:S(2)}) collective-permute-start(bf16[256,768]{1,0:T(8,128)(2,1)S(1)} %broadcast_select_fusion.2.refs_0_), channel_id=1, source_target_pairs={{0,16},{1,17},{2,18},{3,19},{8,24},{9,25},{10,26},{11,27},{4,20},{... | collective-permute-start | bytes 1179656 | tf_op jit(solution)/shard_map/ppermute | solution.py:206
  65.8 36.8 %collective-permute-start.28 = (bf16[256,768]{1,0:T(8,128)(2,1)S(1)}, bf16[256,768]{1,0:T(8,128)(2,1)S(1)}, u32[]{:S(2)}, u32[]{:S(2)}) collective-permute-start(bf16[256,768]{1,0:T(8,128)(2,1)S(1)} %broadcast_select_fusion.1.refs_4_), channel_id=1, source_target_pairs={{0,16},{1,17},{2,18},{3,19},{8,24},{9,25},{10,26},{11,27},{4,20},{... | collective-permute-start | bytes 1179656 | tf_op jit(solution)/shard_map/ppermute | solution.py:206
  78.1 40.8 %copy-start.9 = (bf16[768,256]{1,0:T(8,128)(2,1)S(1)}, bf16[768,256]{1,0:T(8,128)(2,1)}, u32[]{:S(2)}) copy-start(bf16[768,256]{1,0:T(8,128)(2,1)} %param.22) | copy-start | bytes 1179652
  78.1 40.8 %copy-start.11 = (bf16[768,256]{1,0:T(8,128)(2,1)S(1)}, bf16[768,256]{1,0:T(8,128)(2,1)}, u32[]{:S(2)}) copy-start(bf16[768,256]{1,0:T(8,128)(2,1)} %copy-done.10) | copy-start | bytes 1179652
  78.1 36.9 %collective-permute-start.21 = (bf16[192,2048]{1,0:T(8,128)(2,1)S(1)}, bf16[192,2048]{1,0:T(8,128)(2,1)S(1)}, u32[]{:S(2)}, u32[]{:S(2)}) collective-permute-start(bf16[192,2048]{1,0:T(8,128)(2,1)S(1)} %mix.1.own_ref), channel_id=1, source_target_pairs={{0,1},{1,0},{2,3},{3,2},{8,9},{9,8},{10,11},{11,10},{4,5},{5,4},{6... | collective-permute-start | bytes 2359304 | tf_op jit(solution)/shard_map/ppermute | solution.py:206
  78.2 25.8 %collective-permute-start.23 = (bf16[256,768]{1,0:T(8,128)(2,1)S(1)}, bf16[256,768]{1,0:T(8,128)(2,1)S(1)}, u32[]{:S(2)}, u32[]{:S(2)}) collective-permute-start(bf16[256,768]{1,0:T(8,128)(2,1)S(1)} %broadcast_select_fusion.2.refs_0_), channel_id=1, source_target_pairs={{0,4},{1,5},{2,6},{3,7},{8,12},{9,13},{10,14},{11,15},{4,0},{5,1},... | collective-permute-start | bytes 1179656 | tf_op jit(solution)/shard_map/ppermute | solution.py:206
  79.6 24.3 %collective-permute-start.27 = (bf16[256,768]{1,0:T(8,128)(2,1)S(1)}, bf16[256,768]{1,0:T(8,128)(2,1)S(1)}, u32[]{:S(2)}, u32[]{:S(2)}) collective-permute-start(bf16[256,768]{1,0:T(8,128)(2,1)S(1)} %broadcast_select_fusion.1.refs_4_), channel_id=1, source_target_pairs={{0,4},{1,5},{2,6},{3,7},{8,12},{9,13},{10,14},{11,15},{4,0},{5,1},... | collective-permute-start | bytes 1179656 | tf_op jit(solution)/shard_map/ppermute | solution.py:206
  94.1 13.0 %collective-permute-start.25 = (bf16[256,768]{1,0:T(8,128)(2,1)S(1)}, bf16[256,768]{1,0:T(8,128)(2,1)S(1)}, u32[]{:S(2)}, u32[]{:S(2)}) collective-permute-start(bf16[256,768]{1,0:T(8,128)(2,1)S(1)} %collective-permute-done.24.refs_2_), channel_id=1, source_target_pairs={{0,4},{1,5},{2,6},{3,7},{8,12},{9,13},{10,14},{11,15},{4,0},{5,1},... | collective-permute-start | bytes 1179656 | tf_op jit(solution)/shard_map/ppermute | solution.py:206
  102.5 12.4 %collective-permute-start.29 = (bf16[256,768]{1,0:T(8,128)(2,1)S(1)}, bf16[256,768]{1,0:T(8,128)(2,1)S(1)}, u32[]{:S(2)}, u32[]{:S(2)}) collective-permute-start(bf16[256,768]{1,0:T(8,128)(2,1)S(1)} %collective-permute-done.28.refs_6_), channel_id=1, source_target_pairs={{0,4},{1,5},{2,6},{3,7},{8,12},{9,13},{10,14},{11,15},{4,0},{5,1},... | collective-permute-start | bytes 1179656 | tf_op jit(solution)/shard_map/ppermute | solution.py:206
  118.8 31.1 %collective-permute-start.30 = (bf16[384,1536]{1,0:T(8,128)(2,1)S(1)}, bf16[384,1536]{1,0:T(8,128)(2,1)S(1)}, u32[]{:S(2)}, u32[]{:S(2)}) collective-permute-start(bf16[384,1536]{1,0:T(8,128)(2,1)S(1)} %feed_up.1.own_ref), channel_id=1, source_target_pairs={{0,1},{1,0},{2,3},{3,2},{8,9},{9,8},{10,11},{11,10},{4,5},{5,4},{6... | collective-permute-start | bytes 3538952 | tf_op jit(solution)/shard_map/ppermute | solution.py:206
  119.0 19.8 %collective-permute-start.32 = (bf16[768,256]{1,0:T(8,128)(2,1)S(1)}, bf16[768,256]{1,0:T(8,128)(2,1)S(1)}, u32[]{:S(2)}, u32[]{:S(2)}) collective-permute-start(bf16[768,256]{1,0:T(8,128)(2,1)S(1)} %broadcast_select_fusion.refs_0_), channel_id=1, source_target_pairs={{0,16},{1,17},{2,18},{3,19},{8,24},{9,25},{10,26},{11,27},{4,20},{... | collective-permute-start | bytes 1179656 | tf_op jit(solution)/shard_map/ppermute | solution.py:206
  119.2 20.8 %collective-permute-start.31 = (bf16[768,256]{1,0:T(8,128)(2,1)S(1)}, bf16[768,256]{1,0:T(8,128)(2,1)S(1)}, u32[]{:S(2)}, u32[]{:S(2)}) collective-permute-start(bf16[768,256]{1,0:T(8,128)(2,1)S(1)} %broadcast_select_fusion.refs_0_), channel_id=1, source_target_pairs={{0,4},{1,5},{2,6},{3,7},{8,12},{9,13},{10,14},{11,15},{4,0},{5,1},... | collective-permute-start | bytes 1179656 | tf_op jit(solution)/shard_map/ppermute | solution.py:206
  138.8 11.1 %collective-permute-start.33 = (bf16[768,256]{1,0:T(8,128)(2,1)S(1)}, bf16[768,256]{1,0:T(8,128)(2,1)S(1)}, u32[]{:S(2)}, u32[]{:S(2)}) collective-permute-start(bf16[768,256]{1,0:T(8,128)(2,1)S(1)} %collective-permute-done.32.refs_2_), channel_id=1, source_target_pairs={{0,4},{1,5},{2,6},{3,7},{8,12},{9,13},{10,14},{11,15},{4,0},{5,1},... | collective-permute-start | bytes 1179656 | tf_op jit(solution)/shard_map/ppermute | solution.py:206
  153.4 7.8 %collective-permute-start.34 = (bf16[192,512]{1,0:T(8,128)(2,1)S(1)}, bf16[192,512]{1,0:T(8,128)(2,1)S(1)}, u32[]{:S(2)}, u32[]{:S(2)}) collective-permute-start(bf16[192,512]{1,0:T(8,128)(2,1)S(1)} %get-tuple-element.16), channel_id=1, source_target_pairs={{0,8},{1,9},{2,10},{3,11},{8,0},{9,1},{10,2},{11,3},{4,12},{5,13},... | collective-permute-start | bytes 589832 | tf_op jit(solution)/shard_map/ppermute | solution.py:206
  153.5 7.8 %collective-permute-start.35 = (bf16[192,512]{1,0:T(8,128)(2,1)S(1)}, bf16[192,512]{1,0:T(8,128)(2,1)S(1)}, u32[]{:S(2)}, u32[]{:S(2)}) collective-permute-start(bf16[192,512]{1,0:T(8,128)(2,1)S(1)} %get-tuple-element.17), channel_id=1, source_target_pairs={{0,2},{1,3},{2,0},{3,1},{8,10},{9,11},{10,8},{11,9},{4,6},{5,7},{6... | collective-permute-start | bytes 589832 | tf_op jit(solution)/shard_map/ppermute | solution.py:206
  155.0 9.6 %collective-permute-start.36 = (bf16[192,512]{1,0:T(8,128)(2,1)S(1)}, bf16[192,512]{1,0:T(8,128)(2,1)S(1)}, u32[]{:S(2)}, u32[]{:S(2)}) collective-permute-start(bf16[192,512]{1,0:T(8,128)(2,1)S(1)} %get-tuple-element.18), channel_id=1, source_target_pairs={{0,10},{1,11},{2,8},{3,9},{8,2},{9,3},{10,0},{11,1},{4,14},{5,15},... | collective-permute-start | bytes 589832 | tf_op jit(solution)/shard_map/ppermute | solution.py:206
  166.1 1.9 %collective-permute-start.37 = (f32[8,192]{1,0:T(8,128)S(1)}, f32[8,192]{1,0:T(8,128)S(1)}, u32[]{:S(2)}, u32[]{:S(2)}) collective-permute-start(f32[8,192]{1,0:T(8,128)S(1)} %get-tuple-element.20.a_ref), channel_id=1, source_target_pairs={{0,1},{1,0},{2,3},{3,2},{8,9},{9,8},{10,11},{11,10},{4,5},{5,4},{6... | collective-permute-start | bytes 18440 | tf_op jit(solution)/shard_map/ppermute | solution.py:206
  166.1 3.7 %collective-permute-start.38 = (f32[8,192]{1,0:T(8,128)S(1)}, f32[8,192]{1,0:T(8,128)S(1)}, u32[]{:S(2)}, u32[]{:S(2)}) collective-permute-start(f32[8,192]{1,0:T(8,128)S(1)} %get-tuple-element.20.a_ref), channel_id=1, source_target_pairs={{0,2},{1,3},{2,0},{3,1},{8,10},{9,11},{10,8},{11,9},{4,6},{5,7},{6... | collective-permute-start | bytes 18440 | tf_op jit(solution)/shard_map/ppermute | solution.py:206
  166.8 3.1 %collective-permute-start.39 = (f32[8,192]{1,0:T(8,128)S(1)}, f32[8,192]{1,0:T(8,128)S(1)}, u32[]{:S(2)}, u32[]{:S(2)}) collective-permute-start(f32[8,192]{1,0:T(8,128)S(1)} %get-tuple-element.20.a_ref), channel_id=1, source_target_pairs={{0,3},{1,2},{2,1},{3,0},{8,11},{9,10},{10,9},{11,8},{4,7},{5,6},{6... | collective-permute-start | bytes 18440 | tf_op jit(solution)/shard_map/ppermute | solution.py:206
  (9 other events, 44.2 us)
